TPU v7x, 32 devices: a whole 2x2x4 slice. The times are simulated.
32 devices in a mesh: sp: 8 (over z, x), tp: 4 (over y, core).
Axes of the slice: x: 2, y: 2, z: 4, core: 2. Of those that a mesh axis runs over, the one named last changes fastest.
Arguments:
- inputs: bfloat16 [3072, 4096], P('sp', 'tp'), may hold values from -40 to 40, as said below
- query_weight: bfloat16 [2, 4096, 1024], P(None, None, 'tp'), may hold values from -0.2 to 0.2
- key_weight: bfloat16 [2, 4096, 1024], P(None, None, 'tp'), may hold values from -0.2 to 0.2
- value_weight: bfloat16 [4096, 2048], P(None, 'tp'), may hold values from -0.09375 to 0.09375
- pool_weight: bfloat16 [4096, 2048], P(None, 'tp'), may hold values from -0.09375 to 0.09375
- mix_lambda: float32 [16], P('tp'), may hold values from 0.3 to 0.8
- head_gain: float32 [128], replicated, may hold values from 0.1 to 1.9
- attn_out_weight: bfloat16 [2048, 4096], P('tp'), may hold values from -0.125 to 0.125
- pool_out_weight: bfloat16 [2048, 4096], P('tp'), may hold values from -0.125 to 0.125
Outputs:
- mixed: bfloat16 [3072, 4096], P(('sp', 'tp'))
- log_totals: float32 [2, 16, 3072], P(None, 'tp', 'sp')
Inputs may be any that keep to these rules, and one draw needn't show every extreme that they name: inputs of order one, in some draws a few rows larger.
All inputs are finite; a program needn't handle non-finite values.
Results may differ from a plain program's by a relative error of at most 0.015.
Values may be sent and summed in bfloat16 or wider, within the bound.
No kernel may reach another device: no remote copies, remote signals or barrier semaphores. Data moves between devices by JAX's collectives and lax.ppermute only.
A program may use at most 192 MiB of HBM per device.

v0:
```python
import jax
import jax.numpy as jnp
from jax import lax
from jax.experimental import pallas as pl
from jax.experimental.pallas import tpu as pltpu
from jax.sharding import PartitionSpec as P


HEAD_DIM = 64
POOL_WIDTH = 2048
F32 = jnp.float32
BF16 = jnp.bfloat16


LOG_TERMS = 3


def log_rows(rows):
    return -(-2 * LOG_TERMS * rows // (2 * HEAD_DIM) // 16) * 16


def swap(value, axis, offset):
    count = lax.axis_size(axis)
    return lax.ppermute(value, axis, [(i, i ^ offset) for i in range(count)])


def project(pieces, blocks, shaped, plain, first, rank):
    rows, depth = pieces[0].shape
    count, n_shaped = len(pieces), len(shaped)
    half = shaped[0].shape[2] if shaped else 0
    heads = half // HEAD_DIM
    wide = plain.shape[1]
    steps = 2
    sub = depth // steps
    pair = 2 * HEAD_DIM
    acc_shape = jax.ShapeDtypeStruct((rows, 2 * half * n_shaped + wide), F32)

    def body(scalars, *refs):
        x_refs, refs = refs[:count], refs[count:]
        s_refs, refs = refs[: count * n_shaped], refs[count * n_shaped :]
        p_refs, refs = refs[:count], refs[count:]
        if first is not None:
            init, refs = refs[0], refs[1:]
        outs, acc = refs[: len(out_shape)], refs[len(out_shape)]
        step = pl.program_id(0)

        @pl.when(step == 0)
        def _():
            acc[...] = jnp.zeros_like(acc) if first is None else init[...]

        for w in range(n_shaped):
            for m in range(2):
                low = (2 * w + m) * half
                total = acc[:, low : low + half]
                for x_ref, s_ref in zip(x_refs, s_refs[w * count : (w + 1) * count]):
                    total = total + jnp.dot(x_ref[...], s_ref[m], preferred_element_type=F32)
                acc[:, low : low + half] = total
        low = 2 * half * n_shaped
        total = acc[:, low:]
        for x_ref, p_ref in zip(x_refs, p_refs):
            total = total + jnp.dot(x_ref[...], p_ref[...], preferred_element_type=F32)
        acc[:, low:] = total

        @pl.when(step == steps - 1)
        def _():
            if first is None:
                outs[0][...] = acc[...]
            elif not shaped:
                outs[0][...] = acc[...].astype(BF16)
            else:
                hold = refs[-1]
                lead = scalars[count]
                for h in range(heads):
                    key, query = (
                        [acc[:, (2 * w + m) * half + h * HEAD_DIM : (2 * w + m) * half + (h + 1) * HEAD_DIM] for m in range(2)]
                        for w in range(2)
                    )
                    value = [acc[:, low + h * pair : low + (h + 1) * pair]]
                    hold[h ^ lead] = jnp.concatenate(key + value + query, axis=1).astype(BF16)
                for j in range(heads):
                    outs[j][...] = hold[j]
                    outs[heads + j][...] = hold[j, :, : 2 * pair]

    def w_shaped(i):
        return pl.BlockSpec((2, sub, half), lambda k, sc: (0, sc[i] * steps + k, 0))

    def w_plain(i):
        return pl.BlockSpec((sub, wide), lambda k, sc: (sc[i] * steps + k, 0))

    in_specs = [pl.BlockSpec((rows, sub), lambda k, sc: (0, k)) for _ in range(count)]
    in_specs += [w_shaped(i) for _ in shaped for i in range(count)] + [w_plain(i) for i in range(count)]
    args = list(pieces) + [w for w in shaped for _ in range(count)] + [plain] * count
    scratch = [pltpu.VMEM(acc_shape.shape, F32)]
    if first is not None:
        in_specs.append(pl.BlockSpec(acc_shape.shape, lambda k, sc: (0, 0)))
        args.append(first)
    if first is None:
        out_shape = [acc_shape]
    elif not shaped:
        out_shape = [jax.ShapeDtypeStruct((rows, wide), BF16)]
    else:
        out_shape = [jax.ShapeDtypeStruct((rows, 3 * pair), BF16)] * heads
        out_shape += [jax.ShapeDtypeStruct((rows, 2 * pair), BF16)] * heads
        scratch.append(pltpu.VMEM((heads, rows, 3 * pair), BF16))
    out_specs = [pl.BlockSpec(o.shape, lambda k, sc: (0, 0)) for o in out_shape]
    scalars = jnp.stack([b.astype(jnp.int32) for b in blocks] + [rank.astype(jnp.int32)])
    flops = 2 * rows * depth * count * acc_shape.shape[1]
    return pl.pallas_call(
        body,
        grid_spec=pltpu.PrefetchScalarGridSpec(
            num_scalar_prefetch=1, grid=(steps,), in_specs=in_specs, out_specs=out_specs, scratch_shapes=scratch
        ),
        out_shape=out_shape,
        cost_estimate=pl.CostEstimate(flops=flops, bytes_accessed=8 << 20, transcendentals=0),
        compiler_params=pltpu.CompilerParams(vmem_limit_bytes=56 * 2**20),
        name="project",
    )(scalars, *args)


def attend(q, kv, state, lam, gain):
    blocks, rows, width = q.shape
    count = len(kv)
    last = state is not None
    lanes = 2 * HEAD_DIM
    extra = log_rows(rows)

    def body(*refs):
        lam_ref, gain_ref, q_ref, refs = refs[0], refs[1], refs[2], refs[3:]
        kv_refs, refs = refs[:count], refs[count:]
        if last:
            acc_in, max_in, attn_ref = refs
        else:
            acc_out, max_out = refs
        query = q_ref[0] * jnp.asarray(HEAD_DIM ** (-0.5), BF16)
        lane = lax.broadcasted_iota(jnp.int32, (rows, width), 1)
        ones = jnp.ones((kv_refs[0].shape[0], 2 * HEAD_DIM), BF16)
        maps, terms = [], []
        for m in range(2):
            mine = (lane // HEAD_DIM) == m
            query_m = jnp.where(mine, query, jnp.zeros_like(query))
            scores = [
                lax.dot_general(
                    query_m, r[:, : 2 * HEAD_DIM], (((1,), (1,)), ((), ())), preferred_element_type=F32
                )
                for r in kv_refs
            ]
            top = scores[0]
            for s in scores[1:]:
                top = jnp.maximum(top, s)
            top = jnp.max(top, axis=1, keepdims=True)
            if last:
                old = max_in[0, m][:, :1]
                top = jnp.maximum(top, old)
                total = acc_in[0, m] * jnp.exp(old - top)
            else:
                total = None
            for s, r in zip(scores, kv_refs):
                expo = jnp.exp(s - top).astype(BF16)
                side = jnp.concatenate([r[:, 2 * HEAD_DIM : 4 * HEAD_DIM], ones], axis=1)
                add = jnp.dot(expo, side, preferred_element_type=F32)
                total = add if total is None else total + add
            if not last:
                acc_out[0, m] = total
                max_out[0, m] = jnp.broadcast_to(top, (rows, 2 * HEAD_DIM))
            else:
                sums = total[:, 2 * HEAD_DIM :]
                maps.append(total[:, : 2 * HEAD_DIM] / sums)
                logs = jnp.transpose(top + jnp.log(sums))[:1]
                for _ in range(LOG_TERMS):
                    term = logs.astype(BF16)
                    logs = logs - term.astype(F32)
                    terms += [term[:, i : i + lanes].astype(F32) for i in range(0, rows, lanes)]
        if last:
            diff = maps[0] - lam_ref[0] * maps[1]
            norm = lax.rsqrt(jnp.mean(diff * diff, axis=1, keepdims=True) + 1e-05)
            attn_ref[0, :rows] = (diff * norm * gain_ref[...]).astype(BF16)
            terms.append(jnp.zeros((extra - len(terms), lanes), F32))
            attn_ref[0, rows:] = jnp.concatenate(terms, axis=0).astype(BF16)

    whole = 4 * HEAD_DIM
    in_specs = [
        pl.BlockSpec(memory_space=pltpu.SMEM),
        pl.BlockSpec((1, gain.shape[1]), lambda b: (0, 0)),
        pl.BlockSpec((1, rows, width), lambda b: (b, 0, 0)),
    ] + [pl.BlockSpec(a.shape, lambda b: (0, 0)) for a in kv]
    acc_spec = pl.BlockSpec((1, 2, rows, whole), lambda b: (b, 0, 0, 0))
    max_spec = pl.BlockSpec((1, 2, rows, 2 * HEAD_DIM), lambda b: (b, 0, 0, 0))
    args = [lam, gain, q, *kv]
    if last:
        in_specs += [acc_spec, max_spec]
        args += list(state)
        out_shape = [
            jax.ShapeDtypeStruct((blocks, rows + extra, 2 * HEAD_DIM), BF16),
        ]
        out_specs = [
            pl.BlockSpec((1, rows + extra, 2 * HEAD_DIM), lambda b: (b, 0, 0)),
        ]
    else:
        out_shape = [
            jax.ShapeDtypeStruct((blocks, 2, rows, whole), F32),
            jax.ShapeDtypeStruct((blocks, 2, rows, 2 * HEAD_DIM), F32),
        ]
        out_specs = [acc_spec, max_spec]
    pairs = 2 * blocks * rows * count * kv[0].shape[0]
    return pl.pallas_call(
        body,
        grid=(blocks,),
        in_specs=in_specs,
        out_specs=out_specs,
        out_shape=out_shape,
        cost_estimate=pl.CostEstimate(flops=pairs * 12 * HEAD_DIM, bytes_accessed=8 << 20, transcendentals=pairs),
        compiler_params=pltpu.CompilerParams(vmem_limit_bytes=56 * 2**20),
        name="attend",
    )(*args)


def pool(pool_in, before, after):
    tok_rows, channels = pool_in.shape
    padded = jnp.concatenate([before, pool_in, after], axis=0).astype(F32)
    total_tok = tok_rows * lax.axis_size("sp")
    position = lax.axis_index("sp") * tok_rows + jnp.arange(tok_rows, dtype=jnp.int32)
    group = (lax.axis_index("tp") * channels + jnp.arange(channels, dtype=jnp.int32)) // (POOL_WIDTH // 4)
    result = jnp.zeros((tok_rows, channels), F32)
    for group_index, reach in enumerate((2, 4, 8, 16)):
        radius = reach // 2
        window_sum = padded[8 - radius : 8 - radius + tok_rows]
        for shift_by in range(-radius + 1, radius):
            window_sum = window_sum + padded[8 + shift_by : 8 + shift_by + tok_rows]
        low = jnp.clip(position - radius, 0, total_tok)
        high = jnp.clip(position + radius, 0, total_tok)
        window_mean = window_sum / (high - low).astype(F32)[:, None]
        result = jnp.where((group == group_index)[None, :], window_mean, result)
    return (result - pool_in.astype(F32)).astype(BF16)


def on_device(
    inputs,
    query_weight,
    key_weight,
    value_weight,
    pool_weight,
    mix_lambda,
    head_gain,
    attn_out_weight,
    pool_out_weight,
):
    tok_rows = inputs.shape[0]
    heads = query_weight.shape[2] // HEAD_DIM
    n_sp, n_tp = lax.axis_size("sp"), lax.axis_size("tp")
    sp, tp = lax.axis_index("sp"), lax.axis_index("tp")
    rank = sp % heads

    pieces = {0: inputs}
    for offset in range(2, n_tp, 2):
        pieces[offset] = swap(inputs, "tp", offset)
    pieces[1] = swap(inputs, "tp", 1)
    near, far = [0, 1], list(range(2, n_tp))
    place = lambda which: ([pieces[d] for d in which], [tp ^ d for d in which])
    shaped = (key_weight, query_weight)
    (main_sum,) = project(*place(near), shaped, value_weight, None, rank)
    (pool_sum,) = project(*place(near), (), pool_weight, None, rank)
    for offset in range(2, n_tp, 2):
        pieces[offset + 1] = swap(pieces[offset], "tp", 1)
    made = project(*place(far), shaped, value_weight, main_sum, rank)

    own, rest = made[:heads], made[heads:]
    parts = [own[0]] + [swap(own[d], "sp", d) for d in range(1, heads)]
    parts += [swap(rest[d % heads], "sp", d) for d in range(heads, n_sp)]
    (pool_in,) = project(*place(far), (), pool_weight, pool_sum, rank)
    up = [(i, i + 1) for i in range(n_sp - 1)]
    before = lax.ppermute(pool_in[tok_rows - 8 :], "sp", up)
    after = lax.ppermute(pool_in[:8], "sp", [(j, i) for i, j in up])
    pooled = pool(pool_in, before, after)

    lam = lax.dynamic_slice(mix_lambda, (rank,), (1,))
    gain = head_gain[None, :]
    queries = jnp.stack([part[:, 4 * HEAD_DIM :] for part in parts[:heads]])
    state = attend(queries, parts[: n_sp // 2], None, lam, gain)
    (attn,) = attend(queries, parts[n_sp // 2 :], state, lam, gain)

    mine = jnp.zeros((tok_rows, heads * 2 * HEAD_DIM), BF16)
    log_totals = jnp.zeros((2, heads, tok_rows), F32)
    for d in range(heads):
        part = swap(attn[d], "sp", d) if d else attn[d]
        log = part[tok_rows:].reshape(-1)[: 2 * LOG_TERMS * tok_rows].reshape(2, LOG_TERMS, tok_rows)
        log = sum(log[:, i].astype(F32) for i in range(LOG_TERMS))
        mine = lax.dynamic_update_slice(mine, part[:tok_rows], (0, (rank ^ d) * 2 * HEAD_DIM))
        log_totals = lax.dynamic_update_slice(log_totals, log[:, None, :], (0, rank ^ d, 0))

    chip_rows = 2 * tok_rows // n_tp

    def partial(e):
        at = ((tp ^ e) // 2) * chip_rows
        a = lax.dynamic_slice(mine, (at, 0), (chip_rows, mine.shape[1]))
        p = lax.dynamic_slice(pooled, (at, 0), (chip_rows, pooled.shape[1]))
        both = (
            jnp.dot(a, attn_out_weight, preferred_element_type=F32)
            + jnp.dot(p, pool_out_weight, preferred_element_type=F32)
        ).astype(BF16)
        both = lax.optimization_barrier(both.reshape(2, chip_rows // 2, both.shape[1]))
        return (
            lax.dynamic_index_in_dim(both, tp % 2, 0, keepdims=False),
            lax.dynamic_index_in_dim(both, 1 - tp % 2, 0, keepdims=False),
        )

    total = None
    for e in list(range(2, n_tp, 2)) + [0]:
        kept, sent = partial(e)
        pair = kept.astype(F32) + swap(sent, "tp", 1).astype(F32)
        if e:
            pair = swap(pair.astype(BF16), "tp", e).astype(F32)
        total = pair if total is None else total + pair
    return (total.astype(BF16), log_totals)


def solution(mesh):
    in_specs = (
        P("sp", "tp"),
        P(None, None, "tp"),
        P(None, None, "tp"),
        P(None, "tp"),
        P(None, "tp"),
        P("tp"),
        P(),
        P("tp", None),
        P("tp", None),
    )
    out_specs = (P(("sp", "tp"), None), P(None, "tp", "sp"))

    return jax.shard_map(on_device, mesh=mesh, in_specs=in_specs, out_specs=out_specs, check_vma=False)
```

profile of v0, /device:TPU:0, one launch (start us, length us, event | category | flops | bytes accessed | tf_op | source)
XLA Modules:
  0.0 155.9 jit_solution(5306405319852715007)
XLA Ops:
  0.6 3.1 %collective-permute-start = (bf16[384,1024]{1,0:T(8,128)(2,1)}, bf16[384,1024]{1,0:T(8,128)(2,1)S(1)}, u32[]{:S(2)}, u32[]{:S(2)}) collective-permute-start(bf16[384,1024]{1,0:T(8,128)(2,1)} %refs_0_.3), channel_id=1, source_target_pairs={{0,2},{1,3},{2,0},{3,1},{4,6},{5,7},{6,4},{7,5},{8,10},{9,11},{10,... | collective-permute-start | bytes 2359304 | tf_op jit(solution)/shard_map/ppermute | solution.py:24
  3.7 17.8 %collective-permute-done.refs_0_ = bf16[384,1024]{1,0:T(8,128)(2,1)S(1)} collective-permute-done((bf16[384,1024]{1,0:T(8,128)(2,1)}, bf16[384,1024]{1,0:T(8,128)(2,1)S(1)}, u32[]{:S(2)}, u32[]{:S(2)}) %collective-permute-start) | collective-permute-done | bytes 786464 | tf_op jit(solution)/shard_map/ppermute | solution.py:24
  21.6 1.3 dynamic_slice.28.refs_0_
  24.5 4.3 %project.6.refs_4_ = f32[384,512]{1,0:T(8,128)} custom-call(s32[3]{0:T(128)} %get-tuple-element.36.scalars, bf16[384,1024]{1,0:T(8,128)(2,1)} %refs_0_.3, bf16[384,1024]{1,0:T(8,128)(2,1)} %copy-done.5, bf16[4096,512]{1,0:T(8,128)(2,1)} %refs_3_.7, bf16[4096,512]{1,0:T(8,128)(2,1)} %refs_3_.7), custom_call_target="tpu_custom_call" | custom-call | flops 805306368 | bytes 8388608 | tf_op jit(solution)/shard_map/project/pallas_call | solution.py:108
  28.7 7.4 %project.4.refs_8_ = f32[384,1536]{1,0:T(8,128)} custom-call(s32[3]{0:T(128)} %get-tuple-element.36.scalars, bf16[384,1024]{1,0:T(8,128)(2,1)} %refs_0_.3, bf16[384,1024]{1,0:T(8,128)(2,1)} %copy-done.5, bf16[2,4096,256]{2,1,0:T(8,128)(2,1)} %refs_3_.5, bf16[2,4096,256]{2,1,0:T(8,128)(2,1)} %refs_3_.5, bf16[2,4096,256]{2,1,0:T(8,128)(2,1)} %refs_5_.3, ...), custom_call_target="tpu_custom_call" | custom-call | flops 2415919104 | bytes 8388608 | tf_op jit(solution)/shard_map/project/pallas_call | solution.py:108
  37.0 8.4 %project.5 = (bf16[384,384]{1,0:T(8,128)(2,1)}, bf16[384,384]{1,0:T(8,128)(2,1)}, bf16[384,384]{1,0:T(8,128)(2,1)}, bf16[384,384]{1,0:T(8,128)(2,1)}, bf16[384,2...) custom-call(s32[3]{0:T(128)} %get-tuple-element.35.scalars, ...), custom_call_target="tpu_custom_call" | custom-call | flops 2415919104 | bytes 8388608 | tf_op jit(solution)/shard_map/project/pallas_call | solution.py:108
  45.4 2.8 %collective-permute-start.5 = (bf16[384,384]{1,0:T(8,128)(2,1)}, bf16[384,384]{1,0:T(8,128)(2,1)S(1)}, u32[]{:S(2)}, u32[]{:S(2)}) collective-permute-start(bf16[384,384]{1,0:T(8,128)(2,1)} %get-tuple-element.15), channel_id=1, source_target_pairs={{0,12},{4,8},{8,4},{12,0},{16,28},{20,24},{24,20},{28,16},{1,13},{... | collective-permute-start | bytes 884744 | tf_op jit(solution)/shard_map/ppermute | solution.py:24
  48.9 4.6 %project.7 = bf16[384,512]{1,0:T(8,128)(2,1)} custom-call(s32[3]{0:T(128)} %get-tuple-element.35.scalars, bf16[384,1024]{1,0:T(8,128)(2,1)} %copy-done.3, bf16[384,1024]{1,0:T(8,128)(2,1)} %copy-done.4, bf16[4096,512]{1,0:T(8,128)(2,1)} %refs_3_.7, bf16[4096,512]{1,0:T(8,128)(2,1)} %refs_3_.7, f32[384,512]{1,0:T(8,128)} %project.6.refs_4_), custom_call_target="tpu_custom_call" | custom-call | flops 805306368 | bytes 8388608 | tf_op jit(solution)/shard_map/project/pallas_call | solution.py:108
  54.3 3.6 %collective-permute-start.13 = (bf16[8,512]{1,0:T(8,128)(2,1)S(1)}, bf16[8,512]{1,0:T(8,128)(2,1)S(1)}, u32[]{:S(2)}, u32[]{:S(2)}) collective-permute-start(bf16[8,512]{1,0:T(8,128)(2,1)S(1)} %get-tuple-element.25), channel_id=1, source_target_pairs={{0,4},{4,8},{8,12},{12,16},{16,20},{20,24},{24,28},{1,5},{5,9},{9,... | collective-permute-start | bytes 24584 | tf_op jit(solution)/shard_map/ppermute | solution.py:271
  57.9 1.5 collective-permute-start.14
  60.3 1.4 collective-permute-done.13
  61.7 3.3 %collective-permute-start.6 = (bf16[384,256]{1,0:T(8,128)(2,1)S(1)}, bf16[384,256]{1,0:T(8,128)(2,1)S(1)}, u32[]{:S(2)}, u32[]{:S(2)}) collective-permute-start(bf16[384,256]{1,0:T(8,128)(2,1)S(1)} %copy-done.15), channel_id=1, source_target_pairs={{0,16},{4,20},{8,24},{12,28},{16,0},{20,4},{24,8},{28,12},{1,17},{... | collective-permute-start | bytes 589832 | tf_op jit(solution)/shard_map/ppermute | solution.py:24
  65.0 2.9 %collective-permute-start.7 = (bf16[384,256]{1,0:T(8,128)(2,1)S(1)}, bf16[384,256]{1,0:T(8,128)(2,1)S(1)}, u32[]{:S(2)}, u32[]{:S(2)}) collective-permute-start(bf16[384,256]{1,0:T(8,128)(2,1)S(1)} %copy-done.14), channel_id=1, source_target_pairs={{0,20},{4,16},{8,28},{12,24},{16,4},{20,0},{24,12},{28,8},{1,21},{... | collective-permute-start | bytes 589832 | tf_op jit(solution)/shard_map/ppermute | solution.py:24
  67.9 1.1 maximum_convert_fusion
  69.0 3.3 %fusion.16 = bf16[384,512]{1,0:T(8,128)(2,1)S(1)} fusion(bf16[384,512]{1,0:T(8,128)(2,1)} %project.7, f32[400,512]{1,0:T(8,128)S(1)} %maximum_convert_fusion, f32[384]{0:T(512)S(1)} %get-tuple-element.27, f32[384]{0:T(512)S(1)} %get-tuple-element.28, f32[384]{0:T(512)S(1)} %get-tuple-element.29, f32[384]{0:T(512)S(1)} %get-tuple-element.30, ...), kind=kLoop, calls=%fused_computation.29 | loop fusion | flops 7274496 | bytes 13377536 | tf_op jit(solution)/shard_map/convert_element_type | solution.py:233
  72.4 2.6 %fusion.20 = f32[192,4096]{1,0:T(8,128)} fusion(bf16[512,4096]{1,0:T(8,128)(2,1)S(1)} %copy-done, bf16[384,512]{1,0:T(8,128)(2,1)S(1)} %fusion.16, s32[]{:T(128)S(6)} %select_n.104), kind=kOutput, calls=%fused_computation.35 | convolution fusion | flops 805306368 | bytes 7536644 | tf_op jit(solution)/shard_map/dot_general | solution.py:298
  75.0 1.0 fusion.17
  76.0 2.3 %collective-permute-start.8 = (bf16[384,256]{1,0:T(8,128)(2,1)S(1)}, bf16[384,256]{1,0:T(8,128)(2,1)S(1)}, u32[]{:S(2)}, u32[]{:S(2)}) collective-permute-start(bf16[384,256]{1,0:T(8,128)(2,1)S(1)} %copy-done.13), channel_id=1, source_target_pairs={{0,24},{4,28},{8,16},{12,20},{16,8},{20,12},{24,0},{28,4},{1,25},{... | collective-permute-start | bytes 589832 | tf_op jit(solution)/shard_map/ppermute | solution.py:24
  79.9 13.7 %attend.2 = (f32[4,2,384,256]{3,2,1,0:T(8,128)}, f32[4,2,384,128]{3,2,1,0:T(8,128)}) custom-call(f32[1]{0:T(128)} %dynamic_slice.28.refs_0_, f32[1,128]{1,0:T(1,128)} %bitcast.44, bf16[4,384,128]{2,1,0:T(8,128)(2,1)} %pad_maximum_fusion.refs_2_, bf16[384,384]{1,0:T(8,128)(2,1)} %get-tuple-element.12.refs_3_, bf16[384,384]{1,0:T(8,128)(2,1)} %copy-done.10, ...), custom_call_target="tpu_custom_call" | custom-call | flops 3623878656 | bytes 8388608 | tf_op jit(solution)/shard_map/attend/pallas_call | solution.py:205
  94.6 15.9 %attend.3 = bf16[4,416,128]{2,1,0:T(8,128)(2,1)} custom-call(f32[1]{0:T(128)} %dynamic_slice.28.refs_0_, f32[1,128]{1,0:T(1,128)} %bitcast.45, bf16[4,384,128]{2,1,0:T(8,128)(2,1)} %pad_maximum_fusion.refs_2_, bf16[384,256]{1,0:T(8,128)(2,1)} %copy-done.16, bf16[384,256]{1,0:T(8,128)(2,1)} %copy-done.17, bf16[384,256]{1,0:T(8,128)(2,1)} %copy-done.18, ...), custom_call_target="tpu_custom_call" | custom-call | flops 3623878656 | bytes 8388608 | tf_op jit(solution)/shard_map/attend/pallas_call | solution.py:205
  110.5 1.0 slice_bitcast_fusion
  112.2 2.4 %collective-permute-start.10 = (bf16[416,128]{1,0:T(8,128)(2,1)S(1)}, bf16[416,128]{1,0:T(8,128)(2,1)}, u32[]{:S(2)}, u32[]{:S(2)}) collective-permute-start(bf16[416,128]{1,0:T(8,128)(2,1)S(1)} %get-tuple-element.24), channel_id=1, source_target_pairs={{0,4},{4,0},{8,12},{12,8},{16,20},{20,16},{24,28},{28,24},{1,5},{5... | collective-permute-start | bytes 319496 | tf_op jit(solution)/shard_map/ppermute | solution.py:24
  114.7 5.8 %collective-permute-start.11 = (bf16[416,128]{1,0:T(8,128)(2,1)S(1)}, bf16[416,128]{1,0:T(8,128)(2,1)S(1)}, u32[]{:S(2)}, u32[]{:S(2)}) collective-permute-start(bf16[416,128]{1,0:T(8,128)(2,1)S(1)} %get-tuple-element.23), channel_id=1, source_target_pairs={{0,8},{4,12},{8,0},{12,4},{16,24},{20,28},{24,16},{28,20},{1,9},{5... | collective-permute-start | bytes 319496 | tf_op jit(solution)/shard_map/ppermute | solution.py:24
  121.3 0.9 fusion.23
  122.3 0.9 slice_dynamic-update-slice_fusion.2
  123.2 1.0 collective-permute-done.11
  124.2 2.0 %collective-permute-done.12 = bf16[416,128]{1,0:T(8,128)(2,1)S(1)} collective-permute-done((bf16[416,128]{1,0:T(8,128)(2,1)S(1)}, bf16[416,128]{1,0:T(8,128)(2,1)S(1)}, u32[]{:S(2)}, u32[]{:S(2)}) %collective-permute-start.12) | collective-permute-done | bytes 106528 | tf_op jit(solution)/shard_map/ppermute | solution.py:24
  126.9 4.4 %fusion = bf16[192,4096]{1,0:T(8,128)(2,1)S(1)} fusion(f32[192,4096]{1,0:T(8,128)} %fusion.20, bf16[512,4096]{1,0:T(8,128)(2,1)} %param.16, bf16[384,512]{1,0:T(8,128)(2,1)S(1)} %slice_dynamic-update-slice_fusion, s32[]{:T(128)S(6)} %select_n.104), kind=kOutput, calls=%fused_computation.2 | convolution fusion | flops 806879232 | bytes 9109508 | tf_op jit(solution)/shard_map/dot_general | solution.py:297
  131.4 1.1 fusion.1
  133.9 1.6 %collective-permute-start.16 = (bf16[96,4096]{1,0:T(8,128)(2,1)S(1)}, bf16[96,4096]{1,0:T(8,128)(2,1)S(1)}, u32[]{:S(2)}, u32[]{:S(2)}) collective-permute-start(bf16[96,4096]{1,0:T(8,128)(2,1)S(1)} %fusion.4), channel_id=1, source_target_pairs={{0,2},{1,3},{2,0},{3,1},{4,6},{5,7},{6,4},{7,5},{8,10},{9,11},{10,... | collective-permute-start | bytes 2359304 | tf_op jit(solution)/shard_map/ppermute | solution.py:24
  136.5 17.1 %collective-permute-done.16 = bf16[96,4096]{1,0:T(8,128)(2,1)S(1)} collective-permute-done((bf16[96,4096]{1,0:T(8,128)(2,1)S(1)}, bf16[96,4096]{1,0:T(8,128)(2,1)S(1)}, u32[]{:S(2)}, u32[]{:S(2)}) %collective-permute-start.16) | collective-permute-done | bytes 786464 | tf_op jit(solution)/shard_map/ppermute | solution.py:24
  153.6 2.3 %fusion.3 = bf16[96,4096]{1,0:T(8,128)(2,1)} fusion(bf16[96,4096]{1,0:T(8,128)(2,1)S(1)} %collective-permute-done.17, bf16[96,4096]{1,0:T(8,128)(2,1)S(1)} %collective-permute-done.16, bf16[2,96,4096]{2,1,0:T(8,128)(2,1)} %bitcast.43, s32[]{:T(128)S(6)} %select_n.111), kind=kLoop, calls=%fused_computation.6 | loop fusion | flops 2359296 | bytes 3145732 | tf_op jit(solution)/shard_map/convert_element_type | solution.py:313
  (97 shorter events, 12.1 us)
Async XLA Ops:
  0.6 20.8 %collective-permute-start = (bf16[384,1024]{1,0:T(8,128)(2,1)}, bf16[384,1024]{1,0:T(8,128)(2,1)S(1)}, u32[]{:S(2)}, u32[]{:S(2)}) collective-permute-start(bf16[384,1024]{1,0:T(8,128)(2,1)} %refs_0_.3), channel_id=1, source_target_pairs={{0,2},{1,3},{2,0},{3,1},{4,6},{5,7},{6,4},{7,5},{8,10},{9,11},{10,... | collective-permute-start | bytes 2359304 | tf_op jit(solution)/shard_map/ppermute | solution.py:24
  3.7 19.9 %collective-permute-start.2 = (bf16[384,1024]{1,0:T(8,128)(2,1)}, bf16[384,1024]{1,0:T(8,128)(2,1)S(1)}, u32[]{:S(2)}, u32[]{:S(2)}) collective-permute-start(bf16[384,1024]{1,0:T(8,128)(2,1)} %refs_0_.3), channel_id=1, source_target_pairs={{0,1},{1,0},{2,3},{3,2},{4,5},{5,4},{6,7},{7,6},{8,9},{9,8},{10,11... | collective-permute-start | bytes 2359304 | tf_op jit(solution)/shard_map/ppermute | solution.py:24
  21.4 7.3 %copy-start.3 = (bf16[384,1024]{1,0:T(8,128)(2,1)}, bf16[384,1024]{1,0:T(8,128)(2,1)S(1)}, u32[]{:S(2)}) copy-start(bf16[384,1024]{1,0:T(8,128)(2,1)S(1)} %collective-permute-done.refs_0_) | copy-start | bytes 2359300
  21.4 14.7 %collective-permute-start.1 = (bf16[384,1024]{1,0:T(8,128)(2,1)S(1)}, bf16[384,1024]{1,0:T(8,128)(2,1)S(1)}, u32[]{:S(2)}, u32[]{:S(2)}) collective-permute-start(bf16[384,1024]{1,0:T(8,128)(2,1)S(1)} %collective-permute-done.refs_0_), channel_id=1, source_target_pairs={{0,1},{1,0},{2,3},{3,2},{4,5},{5,4},{6,7},{7,6},{8,9},{9,8},{10,11... | collective-permute-start | bytes 2359304 | tf_op jit(solution)/shard_map/ppermute | solution.py:24
  45.4 30.6 %collective-permute-start.5 = (bf16[384,384]{1,0:T(8,128)(2,1)}, bf16[384,384]{1,0:T(8,128)(2,1)S(1)}, u32[]{:S(2)}, u32[]{:S(2)}) collective-permute-start(bf16[384,384]{1,0:T(8,128)(2,1)} %get-tuple-element.15), channel_id=1, source_target_pairs={{0,12},{4,8},{8,4},{12,0},{16,28},{20,24},{24,20},{28,16},{1,13},{... | collective-permute-start | bytes 884744 | tf_op jit(solution)/shard_map/ppermute | solution.py:24
  48.2 30.1 %collective-permute-start.4 = (bf16[384,384]{1,0:T(8,128)(2,1)}, bf16[384,384]{1,0:T(8,128)(2,1)S(1)}, u32[]{:S(2)}, u32[]{:S(2)}) collective-permute-start(bf16[384,384]{1,0:T(8,128)(2,1)} %get-tuple-element.14), channel_id=1, source_target_pairs={{0,8},{4,12},{8,0},{12,4},{16,24},{20,28},{24,16},{28,20},{1,9},{5... | collective-permute-start | bytes 884744 | tf_op jit(solution)/shard_map/ppermute | solution.py:24
  48.6 13.1 %copy-start.15 = (bf16[384,256]{1,0:T(8,128)(2,1)S(1)}, bf16[384,256]{1,0:T(8,128)(2,1)}, u32[]{:S(2)}) copy-start(bf16[384,256]{1,0:T(8,128)(2,1)} %get-tuple-element.16) | copy-start | bytes 589828
  48.6 16.4 %copy-start.14 = (bf16[384,256]{1,0:T(8,128)(2,1)S(1)}, bf16[384,256]{1,0:T(8,128)(2,1)}, u32[]{:S(2)}) copy-start(bf16[384,256]{1,0:T(8,128)(2,1)} %get-tuple-element.17) | copy-start | bytes 589828
  48.6 30.4 %collective-permute-start.3 = (bf16[384,384]{1,0:T(8,128)(2,1)}, bf16[384,384]{1,0:T(8,128)(2,1)S(1)}, u32[]{:S(2)}, u32[]{:S(2)}) collective-permute-start(bf16[384,384]{1,0:T(8,128)(2,1)} %get-tuple-element.13), channel_id=1, source_target_pairs={{0,4},{4,0},{8,12},{12,8},{16,20},{20,16},{24,28},{28,24},{1,5},{5... | collective-permute-start | bytes 884744 | tf_op jit(solution)/shard_map/ppermute | solution.py:24
  54.3 7.4 %collective-permute-start.13 = (bf16[8,512]{1,0:T(8,128)(2,1)S(1)}, bf16[8,512]{1,0:T(8,128)(2,1)S(1)}, u32[]{:S(2)}, u32[]{:S(2)}) collective-permute-start(bf16[8,512]{1,0:T(8,128)(2,1)S(1)} %get-tuple-element.25), channel_id=1, source_target_pairs={{0,4},{4,8},{8,12},{12,16},{16,20},{20,24},{24,28},{1,5},{5,9},{9,... | collective-permute-start | bytes 24584 | tf_op jit(solution)/shard_map/ppermute | solution.py:271
  57.9 7.1 %collective-permute-start.14 = (bf16[8,512]{1,0:T(8,128)(2,1)S(1)}, bf16[8,512]{1,0:T(8,128)(2,1)S(1)}, u32[]{:S(2)}, u32[]{:S(2)}) collective-permute-start(bf16[8,512]{1,0:T(8,128)(2,1)S(1)} %get-tuple-element.26), channel_id=1, source_target_pairs={{4,0},{8,4},{12,8},{16,12},{20,16},{24,20},{28,24},{5,1},{9,5},{13... | collective-permute-start | bytes 24584 | tf_op jit(solution)/shard_map/ppermute | solution.py:272
  61.7 32.0 %collective-permute-start.6 = (bf16[384,256]{1,0:T(8,128)(2,1)S(1)}, bf16[384,256]{1,0:T(8,128)(2,1)S(1)}, u32[]{:S(2)}, u32[]{:S(2)}) collective-permute-start(bf16[384,256]{1,0:T(8,128)(2,1)S(1)} %copy-done.15), channel_id=1, source_target_pairs={{0,16},{4,20},{8,24},{12,28},{16,0},{20,4},{24,8},{28,12},{1,17},{... | collective-permute-start | bytes 589832 | tf_op jit(solution)/shard_map/ppermute | solution.py:24
  65.0 28.6 %collective-permute-start.7 = (bf16[384,256]{1,0:T(8,128)(2,1)S(1)}, bf16[384,256]{1,0:T(8,128)(2,1)S(1)}, u32[]{:S(2)}, u32[]{:S(2)}) collective-permute-start(bf16[384,256]{1,0:T(8,128)(2,1)S(1)} %copy-done.14), channel_id=1, source_target_pairs={{0,20},{4,16},{8,28},{12,24},{16,4},{20,0},{24,12},{28,8},{1,21},{... | collective-permute-start | bytes 589832 | tf_op jit(solution)/shard_map/ppermute | solution.py:24
  69.0 3.4 %copy-start = (bf16[512,4096]{1,0:T(8,128)(2,1)S(1)}, bf16[512,4096]{1,0:T(8,128)(2,1)}, u32[]{:S(2)}) copy-start(bf16[512,4096]{1,0:T(8,128)(2,1)} %param.17) | copy-start | bytes 12582916
  75.0 1.0 copy-start.13
  75.0 3.3 %copy-start.12 = (bf16[384,256]{1,0:T(8,128)(2,1)S(1)}, bf16[384,256]{1,0:T(8,128)(2,1)}, u32[]{:S(2)}) copy-start(bf16[384,256]{1,0:T(8,128)(2,1)} %get-tuple-element.19) | copy-start | bytes 589828
  76.0 3.9 %copy-start.8 = (bf16[384,384]{1,0:T(8,128)(2,1)}, bf16[384,384]{1,0:T(8,128)(2,1)S(1)}, u32[]{:S(2)}) copy-start(bf16[384,384]{1,0:T(8,128)(2,1)S(1)} %collective-permute-done.5.refs_6_) | copy-start | bytes 884740
  76.0 17.6 %collective-permute-start.8 = (bf16[384,256]{1,0:T(8,128)(2,1)S(1)}, bf16[384,256]{1,0:T(8,128)(2,1)S(1)}, u32[]{:S(2)}, u32[]{:S(2)}) collective-permute-start(bf16[384,256]{1,0:T(8,128)(2,1)S(1)} %copy-done.13), channel_id=1, source_target_pairs={{0,24},{4,28},{8,16},{12,20},{16,8},{20,12},{24,0},{28,4},{1,25},{... | collective-permute-start | bytes 589832 | tf_op jit(solution)/shard_map/ppermute | solution.py:24
  78.3 1.6 %copy-start.9 = (bf16[384,384]{1,0:T(8,128)(2,1)}, bf16[384,384]{1,0:T(8,128)(2,1)S(1)}, u32[]{:S(2)}) copy-start(bf16[384,384]{1,0:T(8,128)(2,1)S(1)} %collective-permute-done.4.refs_5_) | copy-start | bytes 884740
  78.3 15.4 %collective-permute-start.9 = (bf16[384,256]{1,0:T(8,128)(2,1)S(1)}, bf16[384,256]{1,0:T(8,128)(2,1)S(1)}, u32[]{:S(2)}, u32[]{:S(2)}) collective-permute-start(bf16[384,256]{1,0:T(8,128)(2,1)S(1)} %copy-done.12), channel_id=1, source_target_pairs={{0,28},{4,24},{8,20},{12,16},{16,12},{20,8},{24,4},{28,0},{1,29},{... | collective-permute-start | bytes 589832 | tf_op jit(solution)/shard_map/ppermute | solution.py:24
  112.2 10.1 %collective-permute-start.10 = (bf16[416,128]{1,0:T(8,128)(2,1)S(1)}, bf16[416,128]{1,0:T(8,128)(2,1)}, u32[]{:S(2)}, u32[]{:S(2)}) collective-permute-start(bf16[416,128]{1,0:T(8,128)(2,1)S(1)} %get-tuple-element.24), channel_id=1, source_target_pairs={{0,4},{4,0},{8,12},{12,8},{16,20},{20,16},{24,28},{28,24},{1,5},{5... | collective-permute-start | bytes 319496 | tf_op jit(solution)/shard_map/ppermute | solution.py:24
  114.7 9.5 %collective-permute-start.11 = (bf16[416,128]{1,0:T(8,128)(2,1)S(1)}, bf16[416,128]{1,0:T(8,128)(2,1)S(1)}, u32[]{:S(2)}, u32[]{:S(2)}) collective-permute-start(bf16[416,128]{1,0:T(8,128)(2,1)S(1)} %get-tuple-element.23), channel_id=1, source_target_pairs={{0,8},{4,12},{8,0},{12,4},{16,24},{20,28},{24,16},{28,20},{1,9},{5... | collective-permute-start | bytes 319496 | tf_op jit(solution)/shard_map/ppermute | solution.py:24
  120.4 5.8 %collective-permute-start.12 = (bf16[416,128]{1,0:T(8,128)(2,1)S(1)}, bf16[416,128]{1,0:T(8,128)(2,1)S(1)}, u32[]{:S(2)}, u32[]{:S(2)}) collective-permute-start(bf16[416,128]{1,0:T(8,128)(2,1)S(1)} %get-tuple-element.22), channel_id=1, source_target_pairs={{0,12},{4,8},{8,4},{12,0},{16,28},{20,24},{24,20},{28,16},{1,13},{... | collective-permute-start | bytes 319496 | tf_op jit(solution)/shard_map/ppermute | solution.py:24
  124.2 2.0 %copy-start.6 = (bf16[416,128]{1,0:T(8,128)(2,1)}, bf16[416,128]{1,0:T(8,128)(2,1)S(1)}, u32[]{:S(2)}) copy-start(bf16[416,128]{1,0:T(8,128)(2,1)S(1)} %collective-permute-done.11) | copy-start | bytes 319492
  126.8 4.5 %copy-start.1 = (bf16[512,4096]{1,0:T(8,128)(2,1)S(1)}, bf16[512,4096]{1,0:T(8,128)(2,1)}, u32[]{:S(2)}) copy-start(bf16[512,4096]{1,0:T(8,128)(2,1)} %param.16) | copy-start | bytes 12582916
  131.3 2.4 %collective-permute-start.15 = (bf16[96,4096]{1,0:T(8,128)(2,1)S(1)}, bf16[96,4096]{1,0:T(8,128)(2,1)S(1)}, u32[]{:S(2)}, u32[]{:S(2)}) collective-permute-start(bf16[96,4096]{1,0:T(8,128)(2,1)S(1)} %dynamic-slice_bitcast_fusion.1), channel_id=1, source_target_pairs={{0,1},{1,0},{2,3},{3,2},{4,5},{5,4},{6,7},{7,6},{8,9},{9,8},{10,11... | collective-permute-start | bytes 2359304 | tf_op jit(solution)/shard_map/ppermute | solution.py:24
  132.5 1.4 copy-start.2
  132.5 3.7 %slice-start = ((bf16[416,128]{1,0:T(8,128)(2,1)}), bf16[18,128]{1,0:T(8,128)(2,1)S(1)}, s32[]{:S(2)}) async-start(bf16[416,128]{1,0:T(8,128)(2,1)} %copy-done.6), calls=%async_computation | async-start | bytes 12288 | tf_op jit(solution)/shard_map/slice | solution.py:285
  132.5 3.7 %slice-start.1 = ((bf16[416,128]{1,0:T(8,128)(2,1)}), bf16[18,128]{1,0:T(8,128)(2,1)S(1)}, s32[]{:S(2)}) async-start(bf16[416,128]{1,0:T(8,128)(2,1)} %copy-done.7), calls=%async_computation.1 | async-start | bytes 12288 | tf_op jit(solution)/shard_map/slice | solution.py:285
  132.6 3.9 %collective-permute-start.17 = (bf16[96,4096]{1,0:T(8,128)(2,1)S(1)}, bf16[96,4096]{1,0:T(8,128)(2,1)S(1)}, u32[]{:S(2)}, u32[]{:S(2)}) collective-permute-start(bf16[96,4096]{1,0:T(8,128)(2,1)S(1)} %dynamic-slice_bitcast_fusion), channel_id=1, source_target_pairs={{0,1},{1,0},{2,3},{3,2},{4,5},{5,4},{6,7},{7,6},{8,9},{9,8},{10,11... | collective-permute-start | bytes 2359304 | tf_op jit(solution)/shard_map/ppermute | solution.py:24
  133.9 19.7 %collective-permute-start.16 = (bf16[96,4096]{1,0:T(8,128)(2,1)S(1)}, bf16[96,4096]{1,0:T(8,128)(2,1)S(1)}, u32[]{:S(2)}, u32[]{:S(2)}) collective-permute-start(bf16[96,4096]{1,0:T(8,128)(2,1)S(1)} %fusion.4), channel_id=1, source_target_pairs={{0,2},{1,3},{2,0},{3,1},{4,6},{5,7},{6,4},{7,5},{8,10},{9,11},{10,... | collective-permute-start | bytes 2359304 | tf_op jit(solution)/shard_map/ppermute | solution.py:24
  136.5 19.4 %copy-start.11 = (f32[2,4,384]{2,1,0:T(4,128)}, f32[2,4,384]{2,1,0:T(4,128)S(1)}, u32[]{:S(2)}) copy-start(f32[2,4,384]{2,1,0:T(4,128)S(1)} %dynamic_update_slice.31) | copy-start | bytes 36868
  (8 other events, 6.5 us)
where the time goes:
time: 157 us; the launch traced here: 156 us
  Pallas kernels  54.3 us (35%)
  waiting for transfers between devices  39.8 us (25%)
  starting transfers between devices  32.2 us (21%)
  local copies, waits for them, and re-layouts  11 us (7%)
  matrix products  9.07 us (6%)
  other arithmetic  8.5 us (5%)
    ppermute x16, waiting for transfers between devices, swap(): return lax.ppermute(value, axis, [(i, i ^ offset) for i in range(count)])  38.4 us
    pallas_call x2, Pallas kernels, attend(): pl.pallas_call(body, grid=(blocks,), in_specs=in_specs, out_specs=out_spe...  29.6 us
    ppermute x16, starting transfers between devices, swap(): return lax.ppermute(value, axis, [(i, i ^ offset) for i in range(count)])  27.1 us
    pallas_call x4, Pallas kernels, project(): pl.pallas_call(body, grid_spec=pltpu.PrefetchScalarGridSpec(num_scalar_pr...  24.6 us
    dot_general x2, matrix products, partial(): jnp.dot(a, attn_out_weight, preferred_element_type=F32)  5.45 us
    dot_general x2, matrix products, partial(): jnp.dot(p, pool_out_weight, preferred_element_type=F32)  3.62 us
    ppermute x1, starting transfers between devices, on_device(): before = lax.ppermute(pool_in[tok_rows - 8:], 'sp', up)  3.6 us
    convert_element_type x1, other arithmetic, pool(): return (result - pool_in.astype(F32)).astype(BF16)  3.34 us
  transfers between devices with their start and end apart: 18, of which 6 were waited for; matrix products, arithmetic and copies ran while one was open for 11% of the time, Pallas kernels for 19%

commit v1 on v0

--- a/solution.py
+++ b/solution.py
@@ -133,32 +133,24 @@
             acc_out, max_out = refs
         query = q_ref[0] * jnp.asarray(HEAD_DIM ** (-0.5), BF16)
         lane = lax.broadcasted_iota(jnp.int32, (rows, width), 1)
-        ones = jnp.ones((kv_refs[0].shape[0], 2 * HEAD_DIM), BF16)
+        keys = jnp.concatenate([r[:, : 2 * HEAD_DIM] for r in kv_refs], axis=0)
+        side = jnp.concatenate([r[:, 2 * HEAD_DIM : 4 * HEAD_DIM] for r in kv_refs], axis=0)
+        side = jnp.concatenate([side, jnp.ones_like(side)], axis=1)
         maps, terms = [], []
         for m in range(2):
             mine = (lane // HEAD_DIM) == m
             query_m = jnp.where(mine, query, jnp.zeros_like(query))
-            scores = [
-                lax.dot_general(
-                    query_m, r[:, : 2 * HEAD_DIM], (((1,), (1,)), ((), ())), preferred_element_type=F32
-                )
-                for r in kv_refs
-            ]
-            top = scores[0]
-            for s in scores[1:]:
-                top = jnp.maximum(top, s)
-            top = jnp.max(top, axis=1, keepdims=True)
+            scores = lax.dot_general(
+                query_m, keys, (((1,), (1,)), ((), ())), preferred_element_type=F32
+            )
+            top = jnp.max(scores, axis=1, keepdims=True)
             if last:
                 old = max_in[0, m][:, :1]
                 top = jnp.maximum(top, old)
-                total = acc_in[0, m] * jnp.exp(old - top)
-            else:
-                total = None
-            for s, r in zip(scores, kv_refs):
-                expo = jnp.exp(s - top).astype(BF16)
-                side = jnp.concatenate([r[:, 2 * HEAD_DIM : 4 * HEAD_DIM], ones], axis=1)
-                add = jnp.dot(expo, side, preferred_element_type=F32)
-                total = add if total is None else total + add
+            expo = jnp.exp(scores - top).astype(BF16)
+            total = jnp.dot(expo, side, preferred_element_type=F32)
+            if last:
+                total = total + acc_in[0, m] * jnp.exp(old - top)
             if not last:
                 acc_out[0, m] = total
                 max_out[0, m] = jnp.broadcast_to(top, (rows, 2 * HEAD_DIM))

time: 157 us -> 154 us (0.981)
  Pallas kernels: 54.3 us -> 49.1 us
  waiting for transfers between devices: 39.8 us -> 41.9 us
    pallas_call x2, Pallas kernels: 29.6 us -> 24.5 us  [attend(): pl.pallas_call(body, grid=(blocks,), in_specs=in_specs, out_specs=out_spe...]
    ppermute x16, waiting for transfers between devices: 38.4 us -> 40.5 us  [swap(): return lax.ppermute(value, axis, [(i, i ^ offset) for i in range(count)])]
  transfers between devices with their start and end apart: 18 -> 18, of which waited for: 6 -> 7; matrix products, arithmetic and copies ran while one was open for 11% -> 11% of each run, Pallas kernels for 19% -> 18%
where the time goes in v1:
time: 154 us; the launch traced here: 153 us
  Pallas kernels  49.1 us (32%)
  waiting for transfers between devices  41.9 us (27%)
  starting transfers between devices  32.6 us (21%)
  local copies, waits for them, and re-layouts  10.9 us (7%)
  matrix products  9.07 us (6%)
  other arithmetic  8.5 us (6%)
    ppermute x16, waiting for transfers between devices, swap(): return lax.ppermute(value, axis, [(i, i ^ offset) for i in range(count)])  40.5 us
    ppermute x16, starting transfers between devices, swap(): return lax.ppermute(value, axis, [(i, i ^ offset) for i in range(count)])  27.5 us
    pallas_call x4, Pallas kernels, project(): pl.pallas_call(body, grid_spec=pltpu.PrefetchScalarGridSpec(num_scalar_pr...  24.6 us
    pallas_call x2, Pallas kernels, attend(): pl.pallas_call(body, grid=(blocks,), in_specs=in_specs, out_specs=out_spe...  24.5 us
    dot_general x2, matrix products, partial(): jnp.dot(a, attn_out_weight, preferred_element_type=F32)  5.45 us
    dot_general x2, matrix products, partial(): jnp.dot(p, pool_out_weight, preferred_element_type=F32)  3.62 us
    ppermute x1, starting transfers between devices, on_device(): before = lax.ppermute(pool_in[tok_rows - 8:], 'sp', up)  3.6 us
    convert_element_type x1, other arithmetic, pool(): return (result - pool_in.astype(F32)).astype(BF16)  3.34 us
  transfers between devices with their start and end apart: 18, of which 7 were waited for; matrix products, arithmetic and copies ran while one was open for 11% of the time, Pallas kernels for 18%

profile of v1, /device:TPU:0, one launch (start us, length us, event | category | flops | bytes accessed | tf_op | source)
XLA Modules:
  0.0 153.2 jit_solution(14227738239033806704)
XLA Ops:
  0.6 3.1 %collective-permute-start = (bf16[384,1024]{1,0:T(8,128)(2,1)}, bf16[384,1024]{1,0:T(8,128)(2,1)S(1)}, u32[]{:S(2)}, u32[]{:S(2)}) collective-permute-start(bf16[384,1024]{1,0:T(8,128)(2,1)} %refs_0_.3), channel_id=1, source_target_pairs={{0,2},{1,3},{2,0},{3,1},{4,6},{5,7},{6,4},{7,5},{8,10},{9,11},{10,... | collective-permute-start | bytes 2359304 | tf_op jit(solution)/shard_map/ppermute | solution.py:24
  3.7 17.8 %collective-permute-done.refs_0_ = bf16[384,1024]{1,0:T(8,128)(2,1)S(1)} collective-permute-done((bf16[384,1024]{1,0:T(8,128)(2,1)}, bf16[384,1024]{1,0:T(8,128)(2,1)S(1)}, u32[]{:S(2)}, u32[]{:S(2)}) %collective-permute-start) | collective-permute-done | bytes 786464 | tf_op jit(solution)/shard_map/ppermute | solution.py:24
  21.6 1.3 dynamic_slice.28.refs_0_
  24.5 4.3 %project.6.refs_4_ = f32[384,512]{1,0:T(8,128)} custom-call(s32[3]{0:T(128)} %get-tuple-element.36.scalars, bf16[384,1024]{1,0:T(8,128)(2,1)} %refs_0_.3, bf16[384,1024]{1,0:T(8,128)(2,1)} %copy-done.5, bf16[4096,512]{1,0:T(8,128)(2,1)} %refs_3_.7, bf16[4096,512]{1,0:T(8,128)(2,1)} %refs_3_.7), custom_call_target="tpu_custom_call" | custom-call | flops 805306368 | bytes 8388608 | tf_op jit(solution)/shard_map/project/pallas_call | solution.py:108
  28.7 7.4 %project.4.refs_8_ = f32[384,1536]{1,0:T(8,128)} custom-call(s32[3]{0:T(128)} %get-tuple-element.36.scalars, bf16[384,1024]{1,0:T(8,128)(2,1)} %refs_0_.3, bf16[384,1024]{1,0:T(8,128)(2,1)} %copy-done.5, bf16[2,4096,256]{2,1,0:T(8,128)(2,1)} %refs_3_.5, bf16[2,4096,256]{2,1,0:T(8,128)(2,1)} %refs_3_.5, bf16[2,4096,256]{2,1,0:T(8,128)(2,1)} %refs_5_.3, ...), custom_call_target="tpu_custom_call" | custom-call | flops 2415919104 | bytes 8388608 | tf_op jit(solution)/shard_map/project/pallas_call | solution.py:108
  37.0 8.4 %project.5 = (bf16[384,384]{1,0:T(8,128)(2,1)}, bf16[384,384]{1,0:T(8,128)(2,1)}, bf16[384,384]{1,0:T(8,128)(2,1)}, bf16[384,384]{1,0:T(8,128)(2,1)}, bf16[384,2...) custom-call(s32[3]{0:T(128)} %get-tuple-element.35.scalars, ...), custom_call_target="tpu_custom_call" | custom-call | flops 2415919104 | bytes 8388608 | tf_op jit(solution)/shard_map/project/pallas_call | solution.py:108
  45.4 2.8 %collective-permute-start.5 = (bf16[384,384]{1,0:T(8,128)(2,1)}, bf16[384,384]{1,0:T(8,128)(2,1)S(1)}, u32[]{:S(2)}, u32[]{:S(2)}) collective-permute-start(bf16[384,384]{1,0:T(8,128)(2,1)} %get-tuple-element.15), channel_id=1, source_target_pairs={{0,12},{4,8},{8,4},{12,0},{16,28},{20,24},{24,20},{28,16},{1,13},{... | collective-permute-start | bytes 884744 | tf_op jit(solution)/shard_map/ppermute | solution.py:24
  48.9 4.6 %project.7 = bf16[384,512]{1,0:T(8,128)(2,1)} custom-call(s32[3]{0:T(128)} %get-tuple-element.35.scalars, bf16[384,1024]{1,0:T(8,128)(2,1)} %copy-done.3, bf16[384,1024]{1,0:T(8,128)(2,1)} %copy-done.4, bf16[4096,512]{1,0:T(8,128)(2,1)} %refs_3_.7, bf16[4096,512]{1,0:T(8,128)(2,1)} %refs_3_.7, f32[384,512]{1,0:T(8,128)} %project.6.refs_4_), custom_call_target="tpu_custom_call" | custom-call | flops 805306368 | bytes 8388608 | tf_op jit(solution)/shard_map/project/pallas_call | solution.py:108
  54.3 3.6 %collective-permute-start.13 = (bf16[8,512]{1,0:T(8,128)(2,1)S(1)}, bf16[8,512]{1,0:T(8,128)(2,1)S(1)}, u32[]{:S(2)}, u32[]{:S(2)}) collective-permute-start(bf16[8,512]{1,0:T(8,128)(2,1)S(1)} %get-tuple-element.25), channel_id=1, source_target_pairs={{0,4},{4,8},{8,12},{12,16},{16,20},{20,24},{24,28},{1,5},{5,9},{9,... | collective-permute-start | bytes 24584 | tf_op jit(solution)/shard_map/ppermute | solution.py:263
  57.9 1.5 collective-permute-start.14
  60.3 1.4 collective-permute-done.13
  61.7 3.3 %collective-permute-start.6 = (bf16[384,256]{1,0:T(8,128)(2,1)S(1)}, bf16[384,256]{1,0:T(8,128)(2,1)S(1)}, u32[]{:S(2)}, u32[]{:S(2)}) collective-permute-start(bf16[384,256]{1,0:T(8,128)(2,1)S(1)} %copy-done.15), channel_id=1, source_target_pairs={{0,16},{4,20},{8,24},{12,28},{16,0},{20,4},{24,8},{28,12},{1,17},{... | collective-permute-start | bytes 589832 | tf_op jit(solution)/shard_map/ppermute | solution.py:24
  65.0 2.9 %collective-permute-start.7 = (bf16[384,256]{1,0:T(8,128)(2,1)S(1)}, bf16[384,256]{1,0:T(8,128)(2,1)S(1)}, u32[]{:S(2)}, u32[]{:S(2)}) collective-permute-start(bf16[384,256]{1,0:T(8,128)(2,1)S(1)} %copy-done.14), channel_id=1, source_target_pairs={{0,20},{4,16},{8,28},{12,24},{16,4},{20,0},{24,12},{28,8},{1,21},{... | collective-permute-start | bytes 589832 | tf_op jit(solution)/shard_map/ppermute | solution.py:24
  67.9 1.1 maximum_convert_fusion
  69.0 3.3 %fusion.16 = bf16[384,512]{1,0:T(8,128)(2,1)S(1)} fusion(bf16[384,512]{1,0:T(8,128)(2,1)} %project.7, f32[400,512]{1,0:T(8,128)S(1)} %maximum_convert_fusion, f32[384]{0:T(512)S(1)} %get-tuple-element.27, f32[384]{0:T(512)S(1)} %get-tuple-element.28, f32[384]{0:T(512)S(1)} %get-tuple-element.29, f32[384]{0:T(512)S(1)} %get-tuple-element.30, ...), kind=kLoop, calls=%fused_computation.29 | loop fusion | flops 7274496 | bytes 13377536 | tf_op jit(solution)/shard_map/convert_element_type | solution.py:225
  72.4 2.6 %fusion.20 = f32[192,4096]{1,0:T(8,128)} fusion(bf16[512,4096]{1,0:T(8,128)(2,1)S(1)} %copy-done, bf16[384,512]{1,0:T(8,128)(2,1)S(1)} %fusion.16, s32[]{:T(128)S(6)} %select_n.104), kind=kOutput, calls=%fused_computation.35 | convolution fusion | flops 805306368 | bytes 7536644 | tf_op jit(solution)/shard_map/dot_general | solution.py:290
  75.0 1.0 fusion.17
  76.0 2.3 %collective-permute-start.8 = (bf16[384,256]{1,0:T(8,128)(2,1)S(1)}, bf16[384,256]{1,0:T(8,128)(2,1)S(1)}, u32[]{:S(2)}, u32[]{:S(2)}) collective-permute-start(bf16[384,256]{1,0:T(8,128)(2,1)S(1)} %copy-done.13), channel_id=1, source_target_pairs={{0,24},{4,28},{8,16},{12,20},{16,8},{20,12},{24,0},{28,4},{1,25},{... | collective-permute-start | bytes 589832 | tf_op jit(solution)/shard_map/ppermute | solution.py:24
  79.9 11.3 %attend.2 = (f32[4,2,384,256]{3,2,1,0:T(8,128)}, f32[4,2,384,128]{3,2,1,0:T(8,128)}) custom-call(f32[1]{0:T(128)} %dynamic_slice.28.refs_0_, f32[1,128]{1,0:T(1,128)} %bitcast.44, bf16[4,384,128]{2,1,0:T(8,128)(2,1)} %pad_maximum_fusion.refs_2_, bf16[384,384]{1,0:T(8,128)(2,1)} %get-tuple-element.12.refs_3_, bf16[384,384]{1,0:T(8,128)(2,1)} %copy-done.10, ...), custom_call_target="tpu_custom_call" | custom-call | flops 3623878656 | bytes 8388608 | tf_op jit(solution)/shard_map/attend/pallas_call | solution.py:197
  91.2 2.1 %collective-permute-done.7.refs_4_ = bf16[384,256]{1,0:T(8,128)(2,1)S(1)} collective-permute-done((bf16[384,256]{1,0:T(8,128)(2,1)S(1)}, bf16[384,256]{1,0:T(8,128)(2,1)S(1)}, u32[]{:S(2)}, u32[]{:S(2)}) %collective-permute-start.7) | collective-permute-done | bytes 196640 | tf_op jit(solution)/shard_map/ppermute | solution.py:24
  94.1 13.2 %attend.3 = bf16[4,416,128]{2,1,0:T(8,128)(2,1)} custom-call(f32[1]{0:T(128)} %dynamic_slice.28.refs_0_, f32[1,128]{1,0:T(1,128)} %bitcast.45, bf16[4,384,128]{2,1,0:T(8,128)(2,1)} %pad_maximum_fusion.refs_2_, bf16[384,256]{1,0:T(8,128)(2,1)} %copy-done.16, bf16[384,256]{1,0:T(8,128)(2,1)} %copy-done.17, bf16[384,256]{1,0:T(8,128)(2,1)} %copy-done.18, ...), custom_call_target="tpu_custom_call" | custom-call | flops 3623878656 | bytes 8388608 | tf_op jit(solution)/shard_map/attend/pallas_call | solution.py:197
  107.4 1.0 slice_bitcast_fusion
  109.5 8.2 %collective-permute-start.11 = (bf16[416,128]{1,0:T(8,128)(2,1)S(1)}, bf16[416,128]{1,0:T(8,128)(2,1)S(1)}, u32[]{:S(2)}, u32[]{:S(2)}) collective-permute-start(bf16[416,128]{1,0:T(8,128)(2,1)S(1)} %get-tuple-element.23), channel_id=1, source_target_pairs={{0,8},{4,12},{8,0},{12,4},{16,24},{20,28},{24,16},{28,20},{1,9},{5... | collective-permute-start | bytes 319496 | tf_op jit(solution)/shard_map/ppermute | solution.py:24
  118.6 0.9 fusion.23
  119.6 0.9 slice_dynamic-update-slice_fusion.2
  120.5 1.0 collective-permute-done.11
  121.5 2.0 %collective-permute-done.12 = bf16[416,128]{1,0:T(8,128)(2,1)S(1)} collective-permute-done((bf16[416,128]{1,0:T(8,128)(2,1)S(1)}, bf16[416,128]{1,0:T(8,128)(2,1)S(1)}, u32[]{:S(2)}, u32[]{:S(2)}) %collective-permute-start.12) | collective-permute-done | bytes 106528 | tf_op jit(solution)/shard_map/ppermute | solution.py:24
  124.2 4.4 %fusion = bf16[192,4096]{1,0:T(8,128)(2,1)S(1)} fusion(f32[192,4096]{1,0:T(8,128)} %fusion.20, bf16[512,4096]{1,0:T(8,128)(2,1)} %param.16, bf16[384,512]{1,0:T(8,128)(2,1)S(1)} %slice_dynamic-update-slice_fusion, s32[]{:T(128)S(6)} %select_n.104), kind=kOutput, calls=%fused_computation.2 | convolution fusion | flops 806879232 | bytes 9109508 | tf_op jit(solution)/shard_map/dot_general | solution.py:289
  128.7 1.1 fusion.1
  131.2 1.6 %collective-permute-start.16 = (bf16[96,4096]{1,0:T(8,128)(2,1)S(1)}, bf16[96,4096]{1,0:T(8,128)(2,1)S(1)}, u32[]{:S(2)}, u32[]{:S(2)}) collective-permute-start(bf16[96,4096]{1,0:T(8,128)(2,1)S(1)} %fusion.4), channel_id=1, source_target_pairs={{0,2},{1,3},{2,0},{3,1},{4,6},{5,7},{6,4},{7,5},{8,10},{9,11},{10,... | collective-permute-start | bytes 2359304 | tf_op jit(solution)/shard_map/ppermute | solution.py:24
  133.8 17.1 %collective-permute-done.16 = bf16[96,4096]{1,0:T(8,128)(2,1)S(1)} collective-permute-done((bf16[96,4096]{1,0:T(8,128)(2,1)S(1)}, bf16[96,4096]{1,0:T(8,128)(2,1)S(1)}, u32[]{:S(2)}, u32[]{:S(2)}) %collective-permute-start.16) | collective-permute-done | bytes 786464 | tf_op jit(solution)/shard_map/ppermute | solution.py:24
  150.9 2.3 %fusion.3 = bf16[96,4096]{1,0:T(8,128)(2,1)} fusion(bf16[96,4096]{1,0:T(8,128)(2,1)S(1)} %collective-permute-done.17, bf16[96,4096]{1,0:T(8,128)(2,1)S(1)} %collective-permute-done.16, bf16[2,96,4096]{2,1,0:T(8,128)(2,1)} %bitcast.43, s32[]{:T(128)S(6)} %select_n.111), kind=kLoop, calls=%fused_computation.6 | loop fusion | flops 2359296 | bytes 3145732 | tf_op jit(solution)/shard_map/convert_element_type | solution.py:305
  (97 shorter events, 12.5 us)
Async XLA Ops:
  0.6 20.8 %collective-permute-start = (bf16[384,1024]{1,0:T(8,128)(2,1)}, bf16[384,1024]{1,0:T(8,128)(2,1)S(1)}, u32[]{:S(2)}, u32[]{:S(2)}) collective-permute-start(bf16[384,1024]{1,0:T(8,128)(2,1)} %refs_0_.3), channel_id=1, source_target_pairs={{0,2},{1,3},{2,0},{3,1},{4,6},{5,7},{6,4},{7,5},{8,10},{9,11},{10,... | collective-permute-start | bytes 2359304 | tf_op jit(solution)/shard_map/ppermute | solution.py:24
  3.7 19.9 %collective-permute-start.2 = (bf16[384,1024]{1,0:T(8,128)(2,1)}, bf16[384,1024]{1,0:T(8,128)(2,1)S(1)}, u32[]{:S(2)}, u32[]{:S(2)}) collective-permute-start(bf16[384,1024]{1,0:T(8,128)(2,1)} %refs_0_.3), channel_id=1, source_target_pairs={{0,1},{1,0},{2,3},{3,2},{4,5},{5,4},{6,7},{7,6},{8,9},{9,8},{10,11... | collective-permute-start | bytes 2359304 | tf_op jit(solution)/shard_map/ppermute | solution.py:24
  21.4 7.3 %copy-start.3 = (bf16[384,1024]{1,0:T(8,128)(2,1)}, bf16[384,1024]{1,0:T(8,128)(2,1)S(1)}, u32[]{:S(2)}) copy-start(bf16[384,1024]{1,0:T(8,128)(2,1)S(1)} %collective-permute-done.refs_0_) | copy-start | bytes 2359300
  21.4 14.7 %collective-permute-start.1 = (bf16[384,1024]{1,0:T(8,128)(2,1)S(1)}, bf16[384,1024]{1,0:T(8,128)(2,1)S(1)}, u32[]{:S(2)}, u32[]{:S(2)}) collective-permute-start(bf16[384,1024]{1,0:T(8,128)(2,1)S(1)} %collective-permute-done.refs_0_), channel_id=1, source_target_pairs={{0,1},{1,0},{2,3},{3,2},{4,5},{5,4},{6,7},{7,6},{8,9},{9,8},{10,11... | collective-permute-start | bytes 2359304 | tf_op jit(solution)/shard_map/ppermute | solution.py:24
  45.4 30.6 %collective-permute-start.5 = (bf16[384,384]{1,0:T(8,128)(2,1)}, bf16[384,384]{1,0:T(8,128)(2,1)S(1)}, u32[]{:S(2)}, u32[]{:S(2)}) collective-permute-start(bf16[384,384]{1,0:T(8,128)(2,1)} %get-tuple-element.15), channel_id=1, source_target_pairs={{0,12},{4,8},{8,4},{12,0},{16,28},{20,24},{24,20},{28,16},{1,13},{... | collective-permute-start | bytes 884744 | tf_op jit(solution)/shard_map/ppermute | solution.py:24
  48.2 30.1 %collective-permute-start.4 = (bf16[384,384]{1,0:T(8,128)(2,1)}, bf16[384,384]{1,0:T(8,128)(2,1)S(1)}, u32[]{:S(2)}, u32[]{:S(2)}) collective-permute-start(bf16[384,384]{1,0:T(8,128)(2,1)} %get-tuple-element.14), channel_id=1, source_target_pairs={{0,8},{4,12},{8,0},{12,4},{16,24},{20,28},{24,16},{28,20},{1,9},{5... | collective-permute-start | bytes 884744 | tf_op jit(solution)/shard_map/ppermute | solution.py:24
  48.6 13.1 %copy-start.15 = (bf16[384,256]{1,0:T(8,128)(2,1)S(1)}, bf16[384,256]{1,0:T(8,128)(2,1)}, u32[]{:S(2)}) copy-start(bf16[384,256]{1,0:T(8,128)(2,1)} %get-tuple-element.16) | copy-start | bytes 589828
  48.6 16.4 %copy-start.14 = (bf16[384,256]{1,0:T(8,128)(2,1)S(1)}, bf16[384,256]{1,0:T(8,128)(2,1)}, u32[]{:S(2)}) copy-start(bf16[384,256]{1,0:T(8,128)(2,1)} %get-tuple-element.17) | copy-start | bytes 589828
  48.6 30.4 %collective-permute-start.3 = (bf16[384,384]{1,0:T(8,128)(2,1)}, bf16[384,384]{1,0:T(8,128)(2,1)S(1)}, u32[]{:S(2)}, u32[]{:S(2)}) collective-permute-start(bf16[384,384]{1,0:T(8,128)(2,1)} %get-tuple-element.13), channel_id=1, source_target_pairs={{0,4},{4,0},{8,12},{12,8},{16,20},{20,16},{24,28},{28,24},{1,5},{5... | collective-permute-start | bytes 884744 | tf_op jit(solution)/shard_map/ppermute | solution.py:24
  54.3 7.4 %collective-permute-start.13 = (bf16[8,512]{1,0:T(8,128)(2,1)S(1)}, bf16[8,512]{1,0:T(8,128)(2,1)S(1)}, u32[]{:S(2)}, u32[]{:S(2)}) collective-permute-start(bf16[8,512]{1,0:T(8,128)(2,1)S(1)} %get-tuple-element.25), channel_id=1, source_target_pairs={{0,4},{4,8},{8,12},{12,16},{16,20},{20,24},{24,28},{1,5},{5,9},{9,... | collective-permute-start | bytes 24584 | tf_op jit(solution)/shard_map/ppermute | solution.py:263
  57.9 7.1 %collective-permute-start.14 = (bf16[8,512]{1,0:T(8,128)(2,1)S(1)}, bf16[8,512]{1,0:T(8,128)(2,1)S(1)}, u32[]{:S(2)}, u32[]{:S(2)}) collective-permute-start(bf16[8,512]{1,0:T(8,128)(2,1)S(1)} %get-tuple-element.26), channel_id=1, source_target_pairs={{4,0},{8,4},{12,8},{16,12},{20,16},{24,20},{28,24},{5,1},{9,5},{13... | collective-permute-start | bytes 24584 | tf_op jit(solution)/shard_map/ppermute | solution.py:264
  61.7 29.5 %collective-permute-start.6 = (bf16[384,256]{1,0:T(8,128)(2,1)S(1)}, bf16[384,256]{1,0:T(8,128)(2,1)S(1)}, u32[]{:S(2)}, u32[]{:S(2)}) collective-permute-start(bf16[384,256]{1,0:T(8,128)(2,1)S(1)} %copy-done.15), channel_id=1, source_target_pairs={{0,16},{4,20},{8,24},{12,28},{16,0},{20,4},{24,8},{28,12},{1,17},{... | collective-permute-start | bytes 589832 | tf_op jit(solution)/shard_map/ppermute | solution.py:24
  65.0 28.3 %collective-permute-start.7 = (bf16[384,256]{1,0:T(8,128)(2,1)S(1)}, bf16[384,256]{1,0:T(8,128)(2,1)S(1)}, u32[]{:S(2)}, u32[]{:S(2)}) collective-permute-start(bf16[384,256]{1,0:T(8,128)(2,1)S(1)} %copy-done.14), channel_id=1, source_target_pairs={{0,20},{4,16},{8,28},{12,24},{16,4},{20,0},{24,12},{28,8},{1,21},{... | collective-permute-start | bytes 589832 | tf_op jit(solution)/shard_map/ppermute | solution.py:24
  69.0 3.4 %copy-start = (bf16[512,4096]{1,0:T(8,128)(2,1)S(1)}, bf16[512,4096]{1,0:T(8,128)(2,1)}, u32[]{:S(2)}) copy-start(bf16[512,4096]{1,0:T(8,128)(2,1)} %param.17) | copy-start | bytes 12582916
  75.0 3.3 %copy-start.12 = (bf16[384,256]{1,0:T(8,128)(2,1)S(1)}, bf16[384,256]{1,0:T(8,128)(2,1)}, u32[]{:S(2)}) copy-start(bf16[384,256]{1,0:T(8,128)(2,1)} %get-tuple-element.19) | copy-start | bytes 589828
  76.0 3.9 %copy-start.8 = (bf16[384,384]{1,0:T(8,128)(2,1)}, bf16[384,384]{1,0:T(8,128)(2,1)S(1)}, u32[]{:S(2)}) copy-start(bf16[384,384]{1,0:T(8,128)(2,1)S(1)} %collective-permute-done.5.refs_6_) | copy-start | bytes 884740
  76.0 17.3 %collective-permute-start.8 = (bf16[384,256]{1,0:T(8,128)(2,1)S(1)}, bf16[384,256]{1,0:T(8,128)(2,1)S(1)}, u32[]{:S(2)}, u32[]{:S(2)}) collective-permute-start(bf16[384,256]{1,0:T(8,128)(2,1)S(1)} %copy-done.13), channel_id=1, source_target_pairs={{0,24},{4,28},{8,16},{12,20},{16,8},{20,12},{24,0},{28,4},{1,25},{... | collective-permute-start | bytes 589832 | tf_op jit(solution)/shard_map/ppermute | solution.py:24
  78.3 1.6 %copy-start.9 = (bf16[384,384]{1,0:T(8,128)(2,1)}, bf16[384,384]{1,0:T(8,128)(2,1)S(1)}, u32[]{:S(2)}) copy-start(bf16[384,384]{1,0:T(8,128)(2,1)S(1)} %collective-permute-done.4.refs_5_) | copy-start | bytes 884740
  78.3 15.0 %collective-permute-start.9 = (bf16[384,256]{1,0:T(8,128)(2,1)S(1)}, bf16[384,256]{1,0:T(8,128)(2,1)S(1)}, u32[]{:S(2)}, u32[]{:S(2)}) collective-permute-start(bf16[384,256]{1,0:T(8,128)(2,1)S(1)} %copy-done.12), channel_id=1, source_target_pairs={{0,28},{4,24},{8,20},{12,16},{16,12},{20,8},{24,4},{28,0},{1,29},{... | collective-permute-start | bytes 589832 | tf_op jit(solution)/shard_map/ppermute | solution.py:24
  91.2 2.1 %copy-start.16 = (bf16[384,256]{1,0:T(8,128)(2,1)}, bf16[384,256]{1,0:T(8,128)(2,1)S(1)}, u32[]{:S(2)}) copy-start(bf16[384,256]{1,0:T(8,128)(2,1)S(1)} %collective-permute-done.6.refs_3_) | copy-start | bytes 589828
  109.1 10.5 %collective-permute-start.10 = (bf16[416,128]{1,0:T(8,128)(2,1)S(1)}, bf16[416,128]{1,0:T(8,128)(2,1)}, u32[]{:S(2)}, u32[]{:S(2)}) collective-permute-start(bf16[416,128]{1,0:T(8,128)(2,1)S(1)} %get-tuple-element.24), channel_id=1, source_target_pairs={{0,4},{4,0},{8,12},{12,8},{16,20},{20,16},{24,28},{28,24},{1,5},{5... | collective-permute-start | bytes 319496 | tf_op jit(solution)/shard_map/ppermute | solution.py:24
  109.5 11.9 %collective-permute-start.11 = (bf16[416,128]{1,0:T(8,128)(2,1)S(1)}, bf16[416,128]{1,0:T(8,128)(2,1)S(1)}, u32[]{:S(2)}, u32[]{:S(2)}) collective-permute-start(bf16[416,128]{1,0:T(8,128)(2,1)S(1)} %get-tuple-element.23), channel_id=1, source_target_pairs={{0,8},{4,12},{8,0},{12,4},{16,24},{20,28},{24,16},{28,20},{1,9},{5... | collective-permute-start | bytes 319496 | tf_op jit(solution)/shard_map/ppermute | solution.py:24
  117.7 5.8 %collective-permute-start.12 = (bf16[416,128]{1,0:T(8,128)(2,1)S(1)}, bf16[416,128]{1,0:T(8,128)(2,1)S(1)}, u32[]{:S(2)}, u32[]{:S(2)}) collective-permute-start(bf16[416,128]{1,0:T(8,128)(2,1)S(1)} %get-tuple-element.22), channel_id=1, source_target_pairs={{0,12},{4,8},{8,4},{12,0},{16,28},{20,24},{24,20},{28,16},{1,13},{... | collective-permute-start | bytes 319496 | tf_op jit(solution)/shard_map/ppermute | solution.py:24
  121.5 2.0 %copy-start.6 = (bf16[416,128]{1,0:T(8,128)(2,1)}, bf16[416,128]{1,0:T(8,128)(2,1)S(1)}, u32[]{:S(2)}) copy-start(bf16[416,128]{1,0:T(8,128)(2,1)S(1)} %collective-permute-done.11) | copy-start | bytes 319492
  124.2 4.5 %copy-start.1 = (bf16[512,4096]{1,0:T(8,128)(2,1)S(1)}, bf16[512,4096]{1,0:T(8,128)(2,1)}, u32[]{:S(2)}) copy-start(bf16[512,4096]{1,0:T(8,128)(2,1)} %param.16) | copy-start | bytes 12582916
  128.6 2.4 %collective-permute-start.15 = (bf16[96,4096]{1,0:T(8,128)(2,1)S(1)}, bf16[96,4096]{1,0:T(8,128)(2,1)S(1)}, u32[]{:S(2)}, u32[]{:S(2)}) collective-permute-start(bf16[96,4096]{1,0:T(8,128)(2,1)S(1)} %dynamic-slice_bitcast_fusion.1), channel_id=1, source_target_pairs={{0,1},{1,0},{2,3},{3,2},{4,5},{5,4},{6,7},{7,6},{8,9},{9,8},{10,11... | collective-permute-start | bytes 2359304 | tf_op jit(solution)/shard_map/ppermute | solution.py:24
  129.8 1.4 copy-start.2
  129.8 3.7 %slice-start = ((bf16[416,128]{1,0:T(8,128)(2,1)}), bf16[18,128]{1,0:T(8,128)(2,1)S(1)}, s32[]{:S(2)}) async-start(bf16[416,128]{1,0:T(8,128)(2,1)} %copy-done.6), calls=%async_computation | async-start | bytes 12288 | tf_op jit(solution)/shard_map/slice | solution.py:277
  129.8 3.7 %slice-start.1 = ((bf16[416,128]{1,0:T(8,128)(2,1)}), bf16[18,128]{1,0:T(8,128)(2,1)S(1)}, s32[]{:S(2)}) async-start(bf16[416,128]{1,0:T(8,128)(2,1)} %copy-done.7), calls=%async_computation.1 | async-start | bytes 12288 | tf_op jit(solution)/shard_map/slice | solution.py:277
  129.9 3.9 %collective-permute-start.17 = (bf16[96,4096]{1,0:T(8,128)(2,1)S(1)}, bf16[96,4096]{1,0:T(8,128)(2,1)S(1)}, u32[]{:S(2)}, u32[]{:S(2)}) collective-permute-start(bf16[96,4096]{1,0:T(8,128)(2,1)S(1)} %dynamic-slice_bitcast_fusion), channel_id=1, source_target_pairs={{0,1},{1,0},{2,3},{3,2},{4,5},{5,4},{6,7},{7,6},{8,9},{9,8},{10,11... | collective-permute-start | bytes 2359304 | tf_op jit(solution)/shard_map/ppermute | solution.py:24
  131.2 19.7 %collective-permute-start.16 = (bf16[96,4096]{1,0:T(8,128)(2,1)S(1)}, bf16[96,4096]{1,0:T(8,128)(2,1)S(1)}, u32[]{:S(2)}, u32[]{:S(2)}) collective-permute-start(bf16[96,4096]{1,0:T(8,128)(2,1)S(1)} %fusion.4), channel_id=1, source_target_pairs={{0,2},{1,3},{2,0},{3,1},{4,6},{5,7},{6,4},{7,5},{8,10},{9,11},{10,... | collective-permute-start | bytes 2359304 | tf_op jit(solution)/shard_map/ppermute | solution.py:24
  133.8 19.4 %copy-start.11 = (f32[2,4,384]{2,1,0:T(4,128)}, f32[2,4,384]{2,1,0:T(4,128)S(1)}, u32[]{:S(2)}) copy-start(f32[2,4,384]{2,1,0:T(4,128)S(1)} %dynamic_update_slice.31) | copy-start | bytes 36868
  (8 other events, 6.6 us)
